TPU v7x, 128 devices: a whole 4x4x4 slice. The times are simulated.
128 devices in a mesh: sp: 32 (over z, y, core), tp: 4 (over x).
Axes of the slice: x: 4, y: 4, z: 4, core: 2. Of those that a mesh axis runs over, the one named last changes fastest.
Arguments:
- queries: bfloat16 [24576, 1024], P('sp', 'tp'), may hold values from -6 to 6
- keys: bfloat16 [24576, 1024], P('sp', 'tp'), may hold values from -6 to 6
- values: bfloat16 [24576, 2048], P('sp', 'tp'), may hold values from -6 to 6
- out_gate: bfloat16 [24576, 2048], P('sp', 'tp'), may hold values from -6 to 6
- input_gates: float32 [2, 4, 24576], P(None, 'tp', 'sp'), may hold values from -4 to 300
- forget_gates: float32 [2, 4, 24576], P(None, 'tp', 'sp'), may hold values from -1 to 16
- doc_ids: int32 [24576], P('sp'), may hold values from 0 to 15, never falling along the last dimension, each value on 1 to 3072 neighbouring positions
- head_gain: float32 [2048], P('tp'), may hold values from 0.1 to 1.9
- w_out: bfloat16 [2048, 2048], P('tp'), may hold values from -0.25 to 0.25
- resid: bfloat16 [24576, 2048], P(('sp', 'tp')), may hold values from -30 to 30
- norm_gain: float32 [2048], replicated, may hold values from 0.1 to 1.9
- w_up: bfloat16 [2048, 8192], P('sp', 'tp'), may hold values from -0.125 to 0.125
- w_down: bfloat16 [8192, 2048], P('tp', 'sp'), may hold values from -0.0625 to 0.0625
Outputs:
- layer_out: bfloat16 [24576, 2048], P(('sp', 'tp'))
Inputs may be any that keep to these rules, and one draw needn't show every extreme that they name: `doc_ids`: document numbers never fall along the positions.
All inputs are finite; a program needn't handle non-finite values.
Results may differ from a plain program's by a relative error of at most 0.013.
Values may be sent and summed in bfloat16 or wider, within the bound.
A program may use at most 128 MiB of HBM per device.

v0:
```python
import jax
import jax.numpy as jnp
from jax import lax
from jax.sharding import Mesh
from jax.sharding import PartitionSpec as P

SP = ("sp_0", "sp_1", "sp_2")
SP_TP = ("sp_0", "sp_1", "sp_2", "tp")
eps = 1e-06
far_low = -1e30


def neutral_like(value, identity):
    return jax.tree.map(
        lambda a, e: jnp.broadcast_to(jnp.asarray(e, a.dtype), a.shape), value, identity
    )


def gathered_once(value, axis):
    leaves = jax.tree.leaves(value)
    turns = sorted(range(len(leaves)), key=lambda k: -leaves[k].size)
    width = (1, *leaves[turns[0]].shape)[-1]
    lines = [
        jnp.pad(leaves[k].reshape(-1), (0, -leaves[k].size % width)).reshape(-1, width)
        for k in turns
    ]
    both, at, found = (lax.all_gather(jnp.concatenate(lines), axis), 0, {})
    for k, line in zip(turns, lines):
        section = both[:, at : at + len(line)].reshape(len(both), -1)
        found[k] = section[:, : leaves[k].size].reshape(-1, *leaves[k].shape)
        at += len(line)
    numbers = iter(range(len(leaves)))
    return jax.tree.map(lambda _: found[next(numbers)], value)


def carried_in(value, axes, combine, identity, reverse):
    before = start = neutral_like(value, identity)
    running = value
    for axis in reversed(axes):
        length, index = (lax.axis_size(axis), lax.axis_index(axis))
        pieces = gathered_once(
            jax.tree.map(
                lambda part, kind: part.astype(kind),
                running,
                jax.tree.map(lambda a: jnp.bfloat16 if a.dtype == jnp.float32 else a.dtype, value),
            ),
            axis,
        )
        inside, running = (start, start)
        for k in reversed(range(length)) if reverse else range(length):
            passed = k > index if reverse else k < index
            running = combine(
                running, jax.tree.map(lambda part, own: part[k].astype(own.dtype), pieces, value)
            )
            inside = jax.tree.map(lambda new, old: jnp.where(passed, new, old), running, inside)
        before = combine(inside, before)
    return before


def split_up(value, dim, length):
    dims = value.shape
    pieces = value.reshape(*dims[:dim], length, dims[dim] // length, *dims[dim + 1 :])
    return jnp.moveaxis(pieces, dim, 0)


def sent_and_summed(value, axis, dim):
    length = lax.axis_size(axis)
    pieces = lax.all_to_all(split_up(value, dim, length), axis, 0, 0, tiled=True)
    return jnp.sum(pieces.astype(jnp.float32), axis=0)


def summarize(keys_blk, values_blk, in_gate, forget_pre, doc_pos):
    logf = jax.nn.log_sigmoid(forget_pre)
    cum = jnp.cumsum(logf)
    length = keys_blk.shape[0]
    last_doc = doc_pos[length - 1]
    tail = doc_pos == last_doc
    total = cum[length - 1]
    exponent = jnp.where(tail, total - cum + in_gate, far_low)
    peak = jnp.max(exponent)
    scaled = jnp.exp(exponent - peak)
    weighted = (keys_blk * scaled[:, None]).astype(jnp.bfloat16)
    memory = jnp.einsum("sd,sv->dv", weighted, values_blk, preferred_element_type=jnp.float32)
    norm_keys = jnp.sum(weighted.astype(jnp.float32), axis=0)
    return (memory, norm_keys, peak, total, doc_pos[0], last_doc, jnp.zeros((), jnp.float32))


def emit(queries_blk, keys_blk, values_blk, in_gate, forget_pre, doc_pos, state):
    memory, norm_keys, top_in, total_in, first_in, last_in, empty_in = state
    scale = queries_blk.shape[1] ** (-0.5)
    logf = jax.nn.log_sigmoid(forget_pre)
    cum = jnp.cumsum(logf)
    length = queries_blk.shape[0]
    place = jnp.arange(length)
    keep = (place[:, None] >= place[None, :]) & (doc_pos[:, None] == doc_pos[None, :])
    exponent = jnp.where(keep, cum[:, None] - cum[None, :] + in_gate[None, :], far_low)
    usable = (doc_pos == last_in) & (empty_in < 0.5)
    carried = jnp.where(usable, cum + top_in, far_low)
    peak = jnp.maximum(carried, jnp.max(exponent, axis=1))
    scores = (
        jnp.einsum("td,sd->ts", queries_blk, keys_blk, preferred_element_type=jnp.float32) * scale
    )
    weights = jnp.where(keep, scores * jnp.exp(exponent - peak[:, None]), 0.0)
    inter = jnp.where(usable, jnp.exp(carried - peak), 0.0)
    query_wide = queries_blk.astype(jnp.float32)
    numer = jnp.dot(weights.astype(jnp.bfloat16), values_blk, preferred_element_type=jnp.float32)
    numer = numer + (inter * scale)[:, None] * jnp.dot(query_wide, memory)
    denom = jnp.sum(weights, axis=1) + inter * scale * jnp.dot(query_wide, norm_keys)
    return numer / jnp.maximum(jnp.abs(denom), 1.0)[:, None]


def combine(early, late):
    e_mem, e_keys, e_top, e_total, e_first, e_last, e_empty = early
    l_mem, l_keys, l_top, l_total, l_first, l_last, l_empty = late
    linked = (l_first == e_last) & (l_first == l_last) & (e_empty < 0.5)
    top = jnp.where(linked, jnp.maximum(l_top, e_top + l_total), l_top)
    early_part = jnp.where(linked, jnp.exp(jnp.minimum(e_top + l_total - top, 0.0)), 0.0)
    late_part = jnp.exp(l_top - top)
    joined = (
        early_part * e_mem + late_part * l_mem,
        early_part * e_keys + late_part * l_keys,
        top,
        e_total + l_total,
        jnp.where(e_empty > 0.5, l_first, e_first),
        l_last,
        jnp.zeros_like(l_empty),
    )
    return tuple((jnp.where(l_empty > 0.5, a, b) for a, b in zip(early, joined)))


def direction(queries3, keys3, values3, in_gates, forget_pre, doc_pos, backward):
    if backward:
        queries3, keys3, values3 = (queries3[::-1], keys3[::-1], values3[::-1])
        in_gates, forget_pre, doc_pos = (in_gates[:, ::-1], forget_pre[:, ::-1], doc_pos[::-1])
    summary = jax.vmap(summarize, in_axes=(1, 1, 0, 0, None))(
        keys3, values3, in_gates, forget_pre, doc_pos
    )
    heads = in_gates.shape[0]
    start = (
        jnp.zeros((heads, keys3.shape[2], values3.shape[2]), jnp.float32),
        jnp.zeros((heads, keys3.shape[2]), jnp.float32),
        jnp.full((heads,), far_low, jnp.float32),
        jnp.zeros((heads,), jnp.float32),
        jnp.full((heads,), -1.0, jnp.float32),
        jnp.full((heads,), -1.0, jnp.float32),
        jnp.ones((heads,), jnp.float32),
    )
    if backward:
        incoming = carried_in(summary, SP, jax.vmap(combine), start, True)
    else:
        incoming = carried_in(summary, SP, jax.vmap(combine), start, False)
    result = jax.vmap(emit, in_axes=(1, 1, 1, 0, 0, None, 0), out_axes=1)(
        queries3, keys3, values3, in_gates, forget_pre, doc_pos, incoming
    )
    if backward:
        result = result[::-1]
    return result


def fetch_weights(w_up, w_down):
    up_full = lax.all_gather(w_up, SP, axis=0, tiled=True)
    down_full = lax.all_gather(w_down, SP, axis=1, tiled=True)
    return (up_full, down_full)


def rms_scale(mixed, norm_gain):
    factor = lax.rsqrt(jnp.mean(mixed * mixed, axis=-1, keepdims=True) + eps)
    return (mixed * factor * norm_gain).astype(jnp.bfloat16)


def shards(
    queries,
    keys,
    values,
    out_gate,
    input_gates,
    forget_gates,
    doc_ids,
    head_gain,
    w_out,
    resid,
    norm_gain,
    w_up,
    w_down,
):
    length = queries.shape[0]
    heads = input_gates.shape[1]
    queries3 = queries.reshape(length, heads, -1)
    keys3 = keys.reshape(length, heads, -1)
    values3 = values.reshape(length, heads, -1)
    doc_pos = doc_ids.astype(jnp.float32)
    memory = direction(queries3, keys3, values3, input_gates[0], forget_gates[0], doc_pos, False)
    memory = memory + direction(
        queries3, keys3, values3, input_gates[1], forget_gates[1], doc_pos, True
    )
    normed = memory * lax.rsqrt(jnp.mean(memory * memory, axis=-1, keepdims=True) + eps)
    gate = jax.nn.sigmoid(out_gate.astype(jnp.float32)).reshape(length, heads, -1)
    readout = (
        (normed * head_gain.reshape(heads, -1) * gate).astype(jnp.bfloat16).reshape(length, -1)
    )
    up_full, down_full = fetch_weights(w_up, w_down)
    picked = readout
    mixed = resid.astype(jnp.float32) + sent_and_summed(
        jnp.dot(picked, w_out, preferred_element_type=jnp.float32).astype(jnp.bfloat16), "tp", 0
    )
    scaled = rms_scale(mixed, norm_gain)
    product = jnp.dot(
        lax.all_gather(scaled, "tp", axis=0, tiled=True),
        up_full,
        preferred_element_type=jnp.float32,
    )
    hidden = jnp.square(jax.nn.relu(product)).astype(jnp.bfloat16)
    picked = hidden
    return (
        mixed
        + sent_and_summed(
            jnp.dot(picked, down_full, preferred_element_type=jnp.float32).astype(jnp.bfloat16),
            "tp",
            0,
        )
    ).astype(jnp.bfloat16)


def solution(mesh):
    split = Mesh(mesh.devices.reshape(4, 4, 2, mesh.shape["tp"]), ("sp_0", "sp_1", "sp_2", "tp"))
    return jax.shard_map(
        shards,
        mesh=split,
        in_specs=(
            P(SP, "tp"),
            P(SP, "tp"),
            P(SP, "tp"),
            P(SP, "tp"),
            P(None, "tp", SP),
            P(None, "tp", SP),
            P(SP),
            P("tp"),
            P("tp", None),
            P(SP_TP, None),
            P(),
            P(SP, "tp"),
            P("tp", SP),
        ),
        out_specs=P(SP_TP, None),
        check_vma=False,
    )
```

profile of v0, /device:TPU:0, one launch (start us, length us, event | category | flops | bytes accessed | tf_op | source)
XLA Modules:
  0.0 496.2 jit_solution(1414788614506800733)
XLA Ops:
  6.5 0.9 negate_reduce_fusion
  8.8 0.7 slice.962
  9.4 0.7 convert_element_type.975
  10.7 0.7 slice_reduce_fusion.2
  13.3 2.1 fusion.304
  16.0 0.6 subtract_exponential_fusion
  16.6 1.2 fusion.204
  17.8 1.9 convolution_convert_fusion.3
  20.6 2.2 all-gather.6
  37.3 1.4 concatenate.19
  38.8 3.8 reverse.15
  42.7 11.9 %reverse.16 = bf16[768,512]{1,0:T(8,128)(2,1)} reverse(bf16[768,512]{1,0:T(8,128)(2,1)} %param.15), dimensions={0} | reverse | bytes 1572864 | tf_op jit(solution)/shard_map/reverse.3
  58.3 1.3 fusion.305
  60.2 0.6 exponential_reduce_fusion
  60.9 1.2 fusion.205
  62.0 1.8 convolution_convert_fusion.2
  64.1 2.2 all-gather.9
  80.7 1.4 concatenate.22
  82.2 1.1 fusion.307
  111.6 1.5 fusion.146
  113.1 1.4 concatenate.20
  114.6 1.1 fusion.309
  144.4 1.5 fusion.147
  145.9 1.4 concatenate.23
  147.7 6.3 %reverse.14 = bf16[768,256]{1,0:T(8,128)(2,1)} reverse(bf16[768,256]{1,0:T(8,128)(2,1)} %param.13), dimensions={0} | reverse | bytes 786432 | tf_op jit(solution)/shard_map/reverse
  154.0 2.3 copy.540
  158.0 1.1 fusion.306
  182.1 1.1 fusion.308
  206.5 2.1 fusion.344
  208.6 2.0 fusion.9
  211.5 1.5 fusion.343
  213.0 0.8 fusion.7
  214.2 4.4 fusion.4
  218.5 13.6 %reverse.17 = f32[768,512]{0,1:T(8,128)} reverse(f32[768,512]{0,1:T(8,128)} %fusion.4), dimensions={0} | reverse | bytes 3145728 | tf_op jit(solution)/shard_map/reverse.5
  232.4 4.4 multiply_reduce_fusion.1
  236.8 2.0 convolution_convert_fusion.1
  238.8 42.3 %all_to_all.10 = bf16[4,192,2048]{2,1,0:T(8,128)(2,1)S(1)} all-to-all(bf16[4,192,2048]{2,1,0:T(8,128)(2,1)S(1)} %bitcast.464), channel_id=1, replica_groups=mesh['sp_0'=4,'sp_1'=4,'sp_2'=2,'tp'=4] {'tp'}, dimensions={0} | all-to-all | bytes 6291456 | tf_op jit(solution)/shard_map/all_to_all | solution.py:68
  282.5 0.8 copy-done.2
  283.4 1.1 multiply_convert_fusion.1
  285.1 0.7 all-gather.24.cloned.1.call-update
  285.8 38.8 %all-gather.20.cloned.1.call-done = bf16[768,2048]{1,0:T(8,128)(2,1)} async-done(((bf16[192,2048]{1,0:T(8,128)(2,1)}), bf16[768,2048]{1,0:T(8,128)(2,1)}) %all-gather.20.cloned.1.call-update) | async-done | bytes 3145744 | tf_op jit(solution)/shard_map/all_gather | solution.py:208
  324.7 55.2 %all-gather.22.cloned.1.call-done = bf16[2048,2048]{1,0:T(8,128)(2,1)} async-done(((bf16[64,2048]{1,0:T(8,128)(2,1)}), bf16[2048,2048]{1,0:T(8,128)(2,1)}) %all-gather.22.cloned.1.call-update) | async-done | bytes 8388624 | tf_op jit(solution)/shard_map/all_gather | solution.py:161
  379.9 11.9 %multiply_convert_fusion = bf16[768,2048]{1,0:T(8,128)(2,1)} fusion(bf16[768,2048]{1,0:T(8,128)(2,1)} %all-gather.20.cloned.1.call-done, bf16[2048,2048]{1,0:T(8,128)(2,1)} %all-gather.22.cloned.1.call-done), kind=kOutput, calls=%fused_computation.1 | convolution fusion | flops 6447169536 | bytes 14680064 | tf_op jit(solution)/shard_map/dot_general | solution.py:207
  391.8 42.8 %all-gather.24.cloned.1.call-done = bf16[2048,2048]{0,1:T(8,128)(2,1)} async-done(((bf16[2048,64]{0,1:T(8,128)(2,1)}), bf16[2048,2048]{0,1:T(8,128)(2,1)}) %all-gather.24.cloned.1.call-update) | async-done | bytes 8388624 | tf_op jit(solution)/shard_map/all_gather | solution.py:162
  434.5 10.1 %convolution_convert_fusion = bf16[768,2048]{1,0:T(8,128)(2,1)S(1)} fusion(bf16[768,2048]{1,0:T(8,128)(2,1)} %multiply_convert_fusion, bf16[2048,2048]{0,1:T(8,128)(2,1)} %all-gather.24.cloned.1.call-done), kind=kOutput, calls=%fused_computation.3 | convolution fusion | flops 6444023808 | bytes 14680064 | tf_op jit(solution)/shard_map/dot_general | solution.py:217
  444.6 42.0 %all_to_all.11 = bf16[4,192,2048]{2,1,0:T(8,128)(2,1)S(1)} all-to-all(bf16[4,192,2048]{2,1,0:T(8,128)(2,1)S(1)} %bitcast.465), channel_id=1, replica_groups=mesh['sp_0'=4,'sp_1'=4,'sp_2'=2,'tp'=4] {'tp'}, dimensions={0} | all-to-all | bytes 6291456 | tf_op jit(solution)/shard_map/all_to_all | solution.py:68
  487.3 0.8 copy-done.3
  488.1 1.2 add_convert_fusion
  (216 shorter events, 28.4 us)
Async XLA Ops:
  6.5 230.3 %copy-start = (bf16[512,2048]{1,0:T(8,128)(2,1)S(1)}, bf16[512,2048]{1,0:T(8,128)(2,1)}, u32[]{:S(2)}) copy-start(bf16[512,2048]{1,0:T(8,128)(2,1)} %param.21) | copy-start | bytes 6291460
  6.5 75.6 %all-gather.26.cloned.1.call-start = ((), (), s32[]{:S(2)}) async-start(), calls=%async_computation.5 | async-start | bytes 1351680 | tf_op jit(solution)/shard_map/all_gather | solution.py:27
  17.8 21.0 %copy-start.5 = (bf16[768,256]{1,0:T(8,128)(2,1)S(1)}, bf16[768,256]{1,0:T(8,128)(2,1)}, u32[]{:S(2)}) copy-start(bf16[768,256]{1,0:T(8,128)(2,1)} %param.14) | copy-start | bytes 1179652
  38.7 75.9 %all-gather.30.cloned.1.call-start = ((), (), s32[]{:S(2)}) async-start(), calls=%async_computation.7 | async-start | bytes 1351680 | tf_op jit(solution)/shard_map/all_gather | solution.py:27
  82.1 75.9 %all-gather.28.cloned.1.call-start = ((), (), s32[]{:S(2)}) async-start(), calls=%async_computation.6 | async-start | bytes 1351680 | tf_op jit(solution)/shard_map/all_gather | solution.py:27
  114.5 67.6 %all-gather.32.cloned.1.call-start = ((), (), s32[]{:S(2)}) async-start(), calls=%async_computation.8 | async-start | bytes 1351680 | tf_op jit(solution)/shard_map/all_gather | solution.py:27
  145.9 60.5 %copy-start.12 = (s32[768]{0:T(1024)S(1)}, s32[768]{0:T(1024)}, u32[]{:S(2)}) copy-start(s32[768]{0:T(1024)} %param.19) | copy-start | bytes 9220
  147.3 177.3 %all-gather.20.cloned.1.call-start = ((), (), s32[]{:S(2)}) async-start(), calls=%async_computation.2 | async-start | bytes 3932160 | tf_op jit(solution)/shard_map/all_gather | solution.py:208
  206.5 2.1 copy-start.9
  208.6 2.9 copy-start.7
  208.6 2.9 copy-start.8
  211.5 1.5 copy-start.10
  218.5 13.6 %copy-start.6 = (bf16[768,256]{1,0:T(8,128)(2,1)S(1)}, bf16[768,256]{1,0:T(8,128)(2,1)}, u32[]{:S(2)}) copy-start(bf16[768,256]{1,0:T(8,128)(2,1)} %param.13) | copy-start | bytes 1179652
  232.4 4.4 copy-start.11
  232.4 4.4 copy-start.14
  281.1 1.1 copy-start.4
  282.2 1.1 copy-start.2
  282.2 1.1 copy-start.13
  284.5 95.4 %all-gather.22.cloned.1.call-start = ((), (), s32[]{:S(2)}) async-start(), calls=%async_computation.3 | async-start | bytes 8650752 | tf_op jit(solution)/shard_map/all_gather | solution.py:161
  285.1 149.5 %all-gather.24.cloned.1.call-start = ((), (), s32[]{:S(2)}) async-start(), calls=%async_computation.4 | async-start | bytes 8650752 | tf_op jit(solution)/shard_map/all_gather | solution.py:162
  486.7 1.4 copy-start.3
  486.7 2.6 copy-start.1
Sparse Core Ops, SparseCore 0:
  38.8 26.7 all-gather.25
  82.2 26.6 all-gather.29
  114.6 26.8 all-gather.27
  147.5 26.8 all-gather.31
  284.6 39.9 all-gather.19
  326.8 53.0 all-gather.21
  382.1 52.3 all-gather.23
where the time goes:
time: 502 us; the launch traced here: 496 us
  waiting for transfers between devices  138 us (27%)
  between operations  134 us (27%)
  blocking collectives  88.7 us (18%)
  local copies, waits for them, and re-layouts  72.9 us (15%)
  matrix products  43.3 us (9%)
  other arithmetic  18.8 us (4%)
    all_to_all x2, blocking collectives, sent_and_summed(): lax.all_to_all(split_up(value, dim, length), axis, 0, 0, tiled=True)  84.3 us
    all_gather x1, waiting for transfers between devices, fetch_weights(): up_full = lax.all_gather(w_up, SP, axis=0, tiled=True)  55.2 us
    all_gather x1, waiting for transfers between devices, fetch_weights(): down_full = lax.all_gather(w_down, SP, axis=1, tiled=True)  42.8 us
    all_gather x1, waiting for transfers between devices, shards(): lax.all_gather(scaled, 'tp', axis=0, tiled=True)  38.8 us
    another operation x7, local copies, waits for them, and re-layouts  35.8 us
    slice x30, local copies, waits for them, and re-layouts, carried_in(): part[k].astype(own.dtype)  17.1 us
    dot_general x1, matrix products, shards(): jnp.dot(lax.all_gather(scaled, 'tp', axis=0, tiled=True), up_full, prefer...  11.9 us
    dot_general x1, matrix products, shards(): jnp.dot(picked, down_full, preferred_element_type=jnp.float32)  10.1 us
  transfers between devices with their start and end apart: 7, of which 3 were waited for; matrix products, arithmetic and copies ran while one was open for 14% of the time, Pallas kernels for 0%

commit v1 on v0

--- a/solution.py
+++ b/solution.py
@@ -8,6 +8,27 @@
 SP_TP = ("sp_0", "sp_1", "sp_2", "tp")
 eps = 1e-06
 far_low = -1e30
+
+
+def in_order(blocks, dim):
+    blocks = jnp.moveaxis(blocks, 0, dim)
+    shape = blocks.shape
+    return blocks.reshape(*shape[:dim], shape[dim] * shape[dim + 1], *shape[dim + 2 :])
+
+
+def collected_by_bits(x, axis):
+    devices, place = (lax.axis_size(axis), lax.axis_index(axis))
+    tiles, apart = (x[None], 1)
+    while apart < devices:
+        other = lax.ppermute(tiles, axis, [(i, i ^ apart) for i in range(devices)])
+        low = place & apart == 0
+        tiles = jnp.concatenate([jnp.where(low, tiles, other), jnp.where(low, other, tiles)])
+        apart *= 2
+    return tiles
+
+
+def collect(value, axis, dim):
+    return in_order(collected_by_bits(value, axis), dim)
 
 
 def neutral_like(value, identity):
@@ -204,11 +225,7 @@
         jnp.dot(picked, w_out, preferred_element_type=jnp.float32).astype(jnp.bfloat16), "tp", 0
     )
     scaled = rms_scale(mixed, norm_gain)
-    product = jnp.dot(
-        lax.all_gather(scaled, "tp", axis=0, tiled=True),
-        up_full,
-        preferred_element_type=jnp.float32,
-    )
+    product = jnp.dot(collect(scaled, "tp", 0), up_full, preferred_element_type=jnp.float32)
     hidden = jnp.square(jax.nn.relu(product)).astype(jnp.bfloat16)
     picked = hidden
     return (

time: 502 us -> 428 us (0.85)
  waiting for transfers between devices: 138 us -> 54.2 us
  other arithmetic: 18.8 us -> 25.2 us
    all_gather x1, waiting for transfers between devices: 55.2 us -> 0.01 us  [fetch_weights(): up_full = lax.all_gather(w_up, SP, axis=0, tiled=True)]
    ppermute x0 -> x2, waiting for transfers between devices: none -> 53 us  [collected_by_bits(): other = lax.ppermute(tiles, axis, [(i, i ^ apart) for i in range(devices)])]
    all_gather x1, waiting for transfers between devices: 42.8 us -> 0.01 us  [fetch_weights(): down_full = lax.all_gather(w_down, SP, axis=1, tiled=True)]
    all_gather x1 -> x0, waiting for transfers between devices: 38.8 us -> none  [shards(): lax.all_gather(scaled, 'tp', axis=0, tiled=True)]
  transfers between devices with their start and end apart: 7 -> 8, of which waited for: 3 -> 2; matrix products, arithmetic and copies ran while one was open for 14% -> 27% of each run, Pallas kernels for 0% -> 0%
where the time goes in v1:
time: 428 us; the launch traced here: 421 us
  between operations  137 us (32%)
  blocking collectives  84.2 us (20%)
  local copies, waits for them, and re-layouts  73.9 us (17%)
  waiting for transfers between devices  54.2 us (13%)
  matrix products  44.3 us (10%)
  other arithmetic  25.2 us (6%)
    all_to_all x2, blocking collectives, sent_and_summed(): lax.all_to_all(split_up(value, dim, length), axis, 0, 0, tiled=True)  79.8 us
    ppermute x2, waiting for transfers between devices, collected_by_bits(): other = lax.ppermute(tiles, axis, [(i, i ^ apart) for i in range(devices)])  53 us
    another operation x7, local copies, waits for them, and re-layouts  36.1 us
    slice x30, local copies, waits for them, and re-layouts, carried_in(): part[k].astype(own.dtype)  17.5 us
    dot_general x1, matrix products, shards(): jnp.dot(collect(scaled, 'tp', 0), up_full, preferred_element_type=jnp.flo...  11.9 us
    dot_general x1, matrix products, shards(): jnp.dot(picked, down_full, preferred_element_type=jnp.float32)  10.1 us
  transfers between devices with their start and end apart: 8, of which 2 were waited for; matrix products, arithmetic and copies ran while one was open for 27% of the time, Pallas kernels for 0%

profile of v1, /device:TPU:0, one launch (start us, length us, event | category | flops | bytes accessed | tf_op | source)
XLA Modules:
  0.0 420.6 jit_solution(1138618671522277722)
XLA Ops:
  6.5 0.9 negate_reduce_fusion
  10.7 0.7 slice_reduce_fusion.2
  13.3 2.1 fusion.305
  16.7 1.2 fusion.205
  17.9 1.9 convolution_convert_fusion.3
  20.6 2.2 all-gather.6
  37.6 1.4 concatenate.25
  39.1 3.8 reverse.15
  43.0 11.9 %reverse.16 = bf16[768,512]{1,0:T(8,128)(2,1)} reverse(bf16[768,512]{1,0:T(8,128)(2,1)} %param.15), dimensions={0} | reverse | bytes 1572864 | tf_op jit(solution)/shard_map/reverse.3
  58.6 1.3 fusion.306
  61.2 1.2 fusion.206
  62.4 1.8 convolution_convert_fusion.2
  64.4 2.2 all-gather.9
  81.9 1.4 concatenate.28
  83.4 1.0 fusion.308
  113.9 1.5 fusion.147
  115.4 1.4 concatenate.26
  116.9 1.1 fusion.310
  147.8 1.5 fusion.148
  149.4 1.4 concatenate.29
  152.0 6.5 %reverse.14 = bf16[768,256]{1,0:T(8,128)(2,1)} reverse(bf16[768,256]{1,0:T(8,128)(2,1)} %param.13), dimensions={0} | reverse | bytes 786432 | tf_op jit(solution)/shard_map/reverse
  158.6 2.3 copy.540
  162.5 1.1 fusion.307
  187.0 1.3 fusion.309
  212.1 1.3 convolution_reduce_fusion
  213.4 2.1 fusion.344
  215.5 0.8 fusion.7
  216.5 4.5 %fusion.4 = f32[768,512]{0,1:T(8,128)} fusion(f32[768,512]{0,1:T(8,128)S(1)} %fusion.7, bf16[768,256]{1,0:T(8,128)(2,1)S(1)} %copy-done.9, f32[768]{0:T(1024)S(1)} %get-tuple-element.16, f32[768]{0:T(1024)S(1)} %get-tuple-element.17, bf16[4,262,512]{2,1,0:T(8,128)(2,1)} %all-gather.29.cloned.1.call-done, f32[]{:T(128)} %bitcast.267, f32[]{:T(128)} %bitcast.266, ...), kind=kOutput, calls=%fused_computation.18 | convolution fusion | flops 210632704 | bytes 6190592 | tf_op jit(solution)/shard_map/vmap()/dot_general | solution.py:128
  221.0 13.6 %reverse.17 = f32[768,512]{0,1:T(8,128)} reverse(f32[768,512]{0,1:T(8,128)} %fusion.4), dimensions={0} | reverse | bytes 3145728 | tf_op jit(solution)/shard_map/reverse.5
  234.7 1.3 convolution_reduce_fusion.1
  236.0 2.6 fusion.345
  238.6 0.8 fusion.9
  240.1 3.4 multiply_reduce_fusion.1
  243.5 2.0 convolution_convert_fusion.1
  245.5 42.0 %all_to_all.10 = bf16[4,192,2048]{2,1,0:T(8,128)(2,1)S(1)} all-to-all(bf16[4,192,2048]{2,1,0:T(8,128)(2,1)S(1)} %bitcast.468), channel_id=1, replica_groups=mesh['sp_0'=4,'sp_1'=4,'sp_2'=2,'tp'=4] {'tp'}, dimensions={0} | all-to-all | bytes 6291456 | tf_op jit(solution)/shard_map/all_to_all | solution.py:89
  289.3 1.1 fusion.11
  291.0 17.9 %collective-permute-done = bf16[1,192,2048]{2,1,0:T(8,128)(2,1)} collective-permute-done((bf16[1,192,2048]{2,1,0:T(8,128)(2,1)}, bf16[1,192,2048]{2,1,0:T(8,128)(2,1)}, u32[]{:S(2)}, u32[]{:S(2)}) %collective-permute-start) | collective-permute-done | bytes 786464 | tf_op jit(solution)/shard_map/ppermute | solution.py:23
  309.0 1.5 broadcast_select_fusion.3
  310.5 1.3 pad_maximum_fusion.1
  311.8 1.0 collective-permute-start.1
  312.7 35.0 %collective-permute-done.1 = bf16[2,192,2048]{2,1,0:T(8,128)(2,1)} collective-permute-done((bf16[2,192,2048]{2,1,0:T(8,128)(2,1)}, bf16[2,192,2048]{2,1,0:T(8,128)(2,1)}, u32[]{:S(2)}, u32[]{:S(2)}) %collective-permute-start.1) | collective-permute-done | bytes 1572896 | tf_op jit(solution)/shard_map/ppermute | solution.py:23
  347.8 1.6 broadcast_select_fusion.1
  349.4 2.0 pad_maximum_fusion
  351.4 11.9 %multiply_convert_fusion = bf16[768,2048]{1,0:T(8,128)(2,1)} fusion(bf16[768,2048]{1,0:T(8,128)(2,1)} %bitcast.467, bf16[2048,2048]{1,0:T(8,128)(2,1)} %all-gather.19.cloned.1.call-done), kind=kOutput, calls=%fused_computation.1 | convolution fusion | flops 6447169536 | bytes 14680064 | tf_op jit(solution)/shard_map/dot_general | solution.py:228
  363.2 10.1 %convolution_convert_fusion = bf16[768,2048]{1,0:T(8,128)(2,1)S(1)} fusion(bf16[768,2048]{1,0:T(8,128)(2,1)} %multiply_convert_fusion, bf16[2048,2048]{0,1:T(8,128)(2,1)} %all-gather.21.cloned.1.call-done), kind=kOutput, calls=%fused_computation.3 | convolution fusion | flops 6444023808 | bytes 14680064 | tf_op jit(solution)/shard_map/dot_general | solution.py:234
  373.3 37.8 %all_to_all.11 = bf16[4,192,2048]{2,1,0:T(8,128)(2,1)S(1)} all-to-all(bf16[4,192,2048]{2,1,0:T(8,128)(2,1)S(1)} %bitcast.469), channel_id=1, replica_groups=mesh['sp_0'=4,'sp_1'=4,'sp_2'=2,'tp'=4] {'tp'}, dimensions={0} | all-to-all | bytes 6291456 | tf_op jit(solution)/shard_map/all_to_all | solution.py:89
  411.7 0.8 copy-done.3
  412.5 1.2 add_convert_fusion
  (223 shorter events, 32.9 us)
Async XLA Ops:
  6.5 236.9 %copy-start = (bf16[512,2048]{1,0:T(8,128)(2,1)S(1)}, bf16[512,2048]{1,0:T(8,128)(2,1)}, u32[]{:S(2)}) copy-start(bf16[512,2048]{1,0:T(8,128)(2,1)} %param.21) | copy-start | bytes 6291460
  6.5 76.9 %all-gather.23.cloned.1.call-start = ((), (), s32[]{:S(2)}) async-start(), calls=%async_computation.4 | async-start | bytes 1351680 | tf_op jit(solution)/shard_map/all_gather | solution.py:48
  17.8 21.3 %copy-start.6 = (bf16[768,256]{1,0:T(8,128)(2,1)S(1)}, bf16[768,256]{1,0:T(8,128)(2,1)}, u32[]{:S(2)}) copy-start(bf16[768,256]{1,0:T(8,128)(2,1)} %param.14) | copy-start | bytes 1179652
  39.0 77.9 %all-gather.27.cloned.1.call-start = ((), (), s32[]{:S(2)}) async-start(), calls=%async_computation.6 | async-start | bytes 1351680 | tf_op jit(solution)/shard_map/all_gather | solution.py:48
  83.3 79.2 %all-gather.25.cloned.1.call-start = ((), (), s32[]{:S(2)}) async-start(), calls=%async_computation.5 | async-start | bytes 1351680 | tf_op jit(solution)/shard_map/all_gather | solution.py:48
  116.9 70.1 %all-gather.29.cloned.1.call-start = ((), (), s32[]{:S(2)}) async-start(), calls=%async_computation.7 | async-start | bytes 1351680 | tf_op jit(solution)/shard_map/all_gather | solution.py:48
  150.8 200.6 %all-gather.19.cloned.1.call-start = ((), (), s32[]{:S(2)}) async-start(), calls=%async_computation.2 | async-start | bytes 8650752 | tf_op jit(solution)/shard_map/all_gather | solution.py:182
  151.4 211.9 %all-gather.21.cloned.1.call-start = ((), (), s32[]{:S(2)}) async-start(), calls=%async_computation.3 | async-start | bytes 8650752 | tf_op jit(solution)/shard_map/all_gather | solution.py:183
  213.4 2.1 copy-start.11
  215.5 1.0 copy-start.9
  221.0 14.9 %copy-start.13 = (s32[768]{0:T(1024)S(1)}, s32[768]{0:T(1024)}, u32[]{:S(2)}) copy-start(s32[768]{0:T(1024)} %param.19) | copy-start | bytes 9220
  221.0 14.9 %copy-start.7 = (bf16[768,256]{1,0:T(8,128)(2,1)S(1)}, bf16[768,256]{1,0:T(8,128)(2,1)}, u32[]{:S(2)}) copy-start(bf16[768,256]{1,0:T(8,128)(2,1)} %param.14) | copy-start | bytes 1179652
  236.0 2.6 copy-start.10
  238.6 1.4 copy-start.5
  238.6 1.5 copy-start.8
  240.1 3.4 copy-start.12
  240.1 3.4 copy-start.15
  287.5 1.1 copy-start.4
  288.6 1.8 copy-start.2
  288.6 0.7 copy-start.14
  290.5 18.5 %collective-permute-start = (bf16[1,192,2048]{2,1,0:T(8,128)(2,1)}, bf16[1,192,2048]{2,1,0:T(8,128)(2,1)}, u32[]{:S(2)}, u32[]{:S(2)}) collective-permute-start(bf16[1,192,2048]{2,1,0:T(8,128)(2,1)} %fusion.11), channel_id=1, source_target_pairs={{0,1},{1,0},{2,3},{3,2},{4,5},{5,4},{6,7},{7,6},{8,9},{9,8},{10,11... | collective-permute-start | bytes 2359304 | tf_op jit(solution)/shard_map/ppermute | solution.py:23
  311.8 36.0 %collective-permute-start.1 = (bf16[2,192,2048]{2,1,0:T(8,128)(2,1)}, bf16[2,192,2048]{2,1,0:T(8,128)(2,1)}, u32[]{:S(2)}, u32[]{:S(2)}) collective-permute-start(bf16[2,192,2048]{2,1,0:T(8,128)(2,1)} %pad_maximum_fusion.1), channel_id=1, source_target_pairs={{0,2},{1,3},{2,0},{3,1},{4,6},{5,7},{6,4},{7,5},{8,10},{9,11},{10,... | collective-permute-start | bytes 4718600 | tf_op jit(solution)/shard_map/ppermute | solution.py:23
  411.1 1.4 copy-start.3
  411.1 2.6 copy-start.1
Sparse Core Ops, SparseCore 0:
  39.1 26.6 all-gather.22
  83.4 26.7 all-gather.26
  117.0 26.8 all-gather.24
  150.9 26.9 all-gather.28
  179.9 53.1 all-gather.18
  235.3 52.3 all-gather.20
